TPU v7x, 32 devices: a whole 2x2x4 slice. The times are simulated.
32 devices in a mesh: fs: 16 (over z, y, x), tp: 2 (over core).
Axes of the slice: x: 2, y: 2, z: 4, core: 2. Of those that a mesh axis runs over, the one named last changes fastest.
Arguments:
- saved_inputs: bfloat16 [2048, 4096], P('fs', 'tp'), may hold values from -6 to 6
- value_cotangent: bfloat16 [2048, 2048], P('fs'), may hold values from -0.1875 to 0.1875
- glu_output: bfloat16 [2048, 2048], P('fs', 'tp'), may hold values from -6 to 6
- conv_cotangent: bfloat16 [2048, 2048], P('fs', 'tp'), may hold values from -0.125 to 0.125
- factor: bfloat16 [4096, 256], P('tp'), may hold values from -0.09375 to 0.09375
- value_weight: float32 [2048, 4096], P('fs', 'tp'), may hold values from -3 to 3
- first_moment: float32 [2048, 256], P('fs', 'tp'), may hold values from -6 to 6
- second_moment: float32 [2048, 256], P('fs', 'tp'), may hold values from 0.25 to 4
- kernel: float32 [31, 2048], P(None, 'tp'), may hold values from -1 to 1
- kernel_first: float32 [31, 2048], P(None, 'tp'), may hold values from -6 to 6
- kernel_second: float32 [31, 2048], P(None, 'tp'), may hold values from 0.25 to 4
Outputs:
- new_value: float32 [2048, 4096], P('fs', 'tp')
- value_copy: bfloat16 [2048, 4096], P('fs', 'tp')
- value_step: float32 [2048, 4096], P('fs', 'tp')
- new_first: float32 [2048, 256], P('fs', 'tp')
- new_second: float32 [2048, 256], P('fs', 'tp')
- new_kernel: float32 [31, 2048], P(None, 'tp')
- new_kernel_first: float32 [31, 2048], P(None, 'tp')
- new_kernel_second: float32 [31, 2048], P(None, 'tp')
All inputs are finite; a program needn't handle non-finite values.
Results may differ from a plain program's by a relative error of at most 0.0055.
Values may be sent and summed in bfloat16 or wider, within the bound.
A program may use at most 64 MiB of HBM per device.

v0:
```python
import jax
import jax.numpy as jnp
from jax import lax
from jax.sharding import PartitionSpec as P

WIDTH = 4096


def from_behind(x, axis, by):
    peers = lax.axis_size(axis)
    pairs = [(i, i + by) for i in range(peers) if 0 <= i + by < peers]
    return lax.ppermute(x, axis, pairs)


def body(
    saved_inputs,
    value_cotangent,
    glu_output,
    conv_cotangent,
    factor,
    value_weight,
    first_moment,
    second_moment,
    kernel,
    kernel_first,
    kernel_second,
):
    highest = lax.Precision.HIGHEST
    factor_f = factor.astype(jnp.float32)
    partial_reduced = jnp.dot(saved_inputs, factor, preferred_element_type=jnp.float32)
    reduced = lax.psum_scatter(
        partial_reduced.astype(jnp.bfloat16), "tp", scatter_dimension=1, tiled=True
    ).astype(jnp.float32)
    upper_part = reduced.astype(jnp.bfloat16)
    lower_part = (reduced - upper_part.astype(jnp.float32)).astype(jnp.bfloat16)
    dims = (((0,), (0,)), ((), ()))
    upper_term = lax.dot_general(
        value_cotangent, upper_part, dims, preferred_element_type=jnp.float32
    )
    lower_term = lax.dot_general(
        value_cotangent, lower_part, dims, preferred_element_type=jnp.float32
    )
    projected = lax.psum_scatter(upper_term + lower_term, "fs", scatter_dimension=0, tiled=True)
    new_first = 0.8 * first_moment + 0.2 * projected
    new_second = 0.9 * second_moment + 0.1 * projected * projected
    direction = new_first / jnp.sqrt(new_second)
    full_direction = lax.all_gather(direction, "tp", axis=1, tiled=True)
    back_proj = jnp.dot(full_direction, factor_f.T, precision=highest)
    row_squares = lax.psum(jnp.sum(back_proj * back_proj, axis=1), "tp")
    value_step = back_proj / jnp.sqrt(row_squares / WIDTH + 0.01)[:, None]
    new_value = value_weight - 0.05 * value_step
    value_copy = new_value.astype(jnp.bfloat16)
    token_count = glu_output.shape[0]
    reach = kernel.shape[0] - 1
    halo_rows = from_behind(glu_output[token_count - reach :], "fs", 1)
    extended = jnp.concatenate([halo_rows, glu_output], axis=0).astype(jnp.float32)
    cotangent_f = conv_cotangent.astype(jnp.float32)
    pieces = []
    for offset in range(kernel.shape[0]):
        begin = reach - offset
        pieces.append(jnp.sum(extended[begin : begin + token_count] * cotangent_f, axis=0))
    local_grad = jnp.stack(pieces, axis=0)
    kernel_grad = lax.psum(local_grad, "fs")
    new_kernel_first = 0.8 * kernel_first + 0.2 * kernel_grad
    new_kernel_second = 0.9 * kernel_second + 0.1 * kernel_grad * kernel_grad
    new_kernel = kernel - 0.05 * new_kernel_first / jnp.sqrt(new_kernel_second)
    return (
        new_value,
        value_copy,
        value_step,
        new_first,
        new_second,
        new_kernel,
        new_kernel_first,
        new_kernel_second,
    )


def solution(mesh):
    placed = (
        P("fs", "tp"),
        P("fs", None),
        P("fs", "tp"),
        P("fs", "tp"),
        P("tp", None),
        P("fs", "tp"),
        P("fs", "tp"),
        P("fs", "tp"),
        P(None, "tp"),
        P(None, "tp"),
        P(None, "tp"),
    )
    return jax.shard_map(
        body,
        mesh=mesh,
        in_specs=placed,
        out_specs=(
            P("fs", "tp"),
            P("fs", "tp"),
            P("fs", "tp"),
            P("fs", "tp"),
            P("fs", "tp"),
            P(None, "tp"),
            P(None, "tp"),
            P(None, "tp"),
        ),
        check_vma=False,
    )
```

profile of v0, /device:TPU:0, one launch (start us, length us, event | category | flops | bytes accessed | tf_op | source)
XLA Modules:
  0.0 225.3 jit_solution(7543839092658024599)
XLA Ops:
  8.0 0.0 reduce-scatter.7.cloned.1.call-start
  8.1 0.9 slice.96
  9.0 4.9 %collective-permute-start = (bf16[30,1024]{1,0:T(8,128)(2,1)S(1)}, bf16[30,1024]{1,0:T(8,128)(2,1)S(1)}, u32[]{:S(2)}, u32[]{:S(2)}) collective-permute-start(bf16[30,1024]{1,0:T(8,128)(2,1)S(1)} %slice.96), channel_id=1, source_target_pairs={{0,2},{2,4},{4,6},{6,8},{8,10},{10,12},{12,14},{14,16},{16,18},{18... | collective-permute-start | bytes 184328 | tf_op jit(solution)/shard_map/ppermute | solution.py:12
  13.9 1.4 convolution_convert_fusion
  15.3 0.7 copy.27
  16.0 0.0 reduce-scatter.7.cloned.1.call-update
  16.1 0.0 all-reduce.2.cloned.1.call-start
  16.1 0.1 maximum_convert_fusion
  16.2 0.8 copy-done.3
  17.0 1.1 fusion.31
  18.1 0.8 fusion.30
  18.9 2.7 %stack.127 = f32[31,1024]{1,0:T(8,128)} concatenate(f32[1,1024]{1,0:T(1,128)S(1)} %bitcast.75, f32[1,1024]{1,0:T(1,128)S(1)} %bitcast.46, f32[1,1024]{1,0:T(1,128)S(1)} %bitcast.47, f32[1,1024]{1,0:T(1,128)S(1)} %bitcast.48, f32[1,1024]{1,0:T(1,128)S(1)} %bitcast.49, f32[1,1024]{1,0:T(1,128)S(1)} %bitcast.50, f32[1,1024]{1,0:T(1,128)S(1)} %bitcast.51, f32[1,1024]{1,0:T(1,128)S(1)} %bitcast.52, ...), dimensions={0} | concatenate | bytes 253952 | tf_op jit(solution)/shard_map/stack | solution.py:62
  21.6 0.0 all-reduce.2.cloned.1.call-update
  21.6 0.0 reduce-scatter.5.cloned.1.call-start
  21.7 2.4 %reduce-scatter.7.cloned.1.call-done = bf16[128,128]{1,0:T(8,128)(2,1)} async-done(((bf16[256,128]{1,0:T(8,128)(2,1)}), bf16[128,128]{1,0:T(8,128)(2,1)}) %reduce-scatter.7.cloned.1.call-update) | async-done | bytes 32784
  24.1 0.9 copy.28
  25.0 0.3 fusion.34
  25.3 1.3 fusion
  26.6 0.0 reduce-scatter.5.cloned.1.call-update
  26.6 0.8 copy-done.9
  27.5 0.1 copy.24
  27.6 0.1 copy.23
  27.7 100.1 %all-reduce.2.cloned.1.call-done = f32[31,1024]{1,0:T(8,128)} async-done(((f32[31,1024]{1,0:T(8,128)}), f32[31,1024]{1,0:T(8,128)}) %all-reduce.2.cloned.1.call-update) | async-done | bytes 126992 | tf_op jit(solution)/shard_map/psum | solution.py:63
  127.7 1.7 multiply_subtract_fusion.1
  129.4 78.8 %reduce-scatter.5.cloned.1.call-done = f32[128,128]{0,1:T(8,128)} async-done(((f32[2048,128]{0,1:T(8,128)}), f32[128,128]{0,1:T(8,128)}) %reduce-scatter.5.cloned.1.call-update) | async-done | bytes 65552 | tf_op jit(solution)/shard_map/reduce_scatter | solution.py:43
  208.2 0.9 rsqrt_multiply_fusion
  209.1 1.9 all_gather.3
  211.0 1.1 multiply_reduce_fusion
  212.1 2.5 %psum.14 = f32[128]{0:T(128)S(1)} all-reduce(f32[128]{0:T(128)S(1)} %get-tuple-element.64), channel_id=1, replica_groups=mesh['fs'=16,'tp'=2] {'tp'}, use_global_device_ids=true, to_apply=%region_3.0 | all-reduce | flops 128 | bytes 1024 | tf_op jit(solution)/shard_map/psum | solution.py:49
  214.5 0.7 copy.25
  215.3 0.7 copy.26
  216.0 1.8 fusion.37
  (22 shorter events, 0.1 us)
Async XLA Ops:
  8.0 5.9 %copy-start = (bf16[2048,256]{1,0:T(8,128)(2,1)S(1)}, bf16[2048,256]{1,0:T(8,128)(2,1)}, u32[]{:S(2)}) copy-start(bf16[2048,256]{1,0:T(8,128)(2,1)} %param.15) | copy-start | bytes 3145732
  8.0 16.1 %reduce-scatter.7.cloned.1.call-start = ((), (), s32[]{:S(2)}) async-start(), calls=%async_computation.4 | async-start | bytes 98304
  9.0 7.1 %collective-permute-start = (bf16[30,1024]{1,0:T(8,128)(2,1)S(1)}, bf16[30,1024]{1,0:T(8,128)(2,1)S(1)}, u32[]{:S(2)}, u32[]{:S(2)}) collective-permute-start(bf16[30,1024]{1,0:T(8,128)(2,1)S(1)} %slice.96), channel_id=1, source_target_pairs={{0,2},{2,4},{4,6},{6,8},{8,10},{10,12},{12,14},{14,16},{16,18},{18... | collective-permute-start | bytes 184328 | tf_op jit(solution)/shard_map/ppermute | solution.py:12
  13.9 2.2 copy-start.4
  16.1 1.0 copy-start.3
  16.1 111.7 %all-reduce.2.cloned.1.call-start = ((), (), s32[]{:S(2)}) async-start(), calls=%async_computation.3 | async-start | bytes 262144 | tf_op jit(solution)/shard_map/psum | solution.py:63
  18.9 6.1 %copy-start.1 = (bf16[128,2048]{1,0:T(8,128)(2,1)S(1)}, bf16[128,2048]{1,0:T(8,128)(2,1)}, u32[]{:S(2)}) copy-start(bf16[128,2048]{1,0:T(8,128)(2,1)} %param.12) | copy-start | bytes 1572868
  21.6 186.6 %reduce-scatter.5.cloned.1.call-start = ((), (), s32[]{:S(2)}) async-start(), calls=%async_computation.2 | async-start | bytes 1114112 | tf_op jit(solution)/shard_map/reduce_scatter | solution.py:43
  24.1 1.0 copy-start.8
  26.6 0.8 copy-start.9
  26.6 0.9 copy-start.10
  26.6 101.1 %copy-start.7 = (f32[31,1024]{1,0:T(8,128)S(1)}, f32[31,1024]{1,0:T(8,128)}, u32[]{:S(2)}) copy-start(f32[31,1024]{1,0:T(8,128)} %param.21) | copy-start | bytes 380932
  27.5 100.3 %copy-start.5 = (f32[31,1024]{1,0:T(8,128)S(1)}, f32[31,1024]{1,0:T(8,128)}, u32[]{:S(2)}) copy-start(f32[31,1024]{1,0:T(8,128)} %param.19) | copy-start | bytes 380932
  27.5 100.3 %copy-start.6 = (f32[31,1024]{1,0:T(8,128)S(1)}, f32[31,1024]{1,0:T(8,128)}, u32[]{:S(2)}) copy-start(f32[31,1024]{1,0:T(8,128)} %param.20) | copy-start | bytes 380932
  211.0 5.0 %copy-start.2 = (f32[128,2048]{1,0:T(8,128)S(1)}, f32[128,2048]{1,0:T(8,128)}, u32[]{:S(2)}) copy-start(f32[128,2048]{1,0:T(8,128)} %param.16) | copy-start | bytes 3145732
Sparse Core Ops, SparseCore 0:
  16.2 7.8 reduce-scatter.6
Sparse Core Ops, SparseCore 1:
  22.6 105.1 all-reduce.1
  130.4 77.7 reduce-scatter.4
where the time goes:
time: 226 us; the launch traced here: 225 us
  waiting for transfers between devices  181 us (80%)
  between operations  15.6 us (7%)
  local copies, waits for them, and re-layouts  8.54 us (4%)
  other arithmetic  6.33 us (3%)
  starting transfers between devices  5 us (2%)
  blocking collectives  4.37 us (2%)
  matrix products  4.05 us (2%)
    psum x1, waiting for transfers between devices, body(): kernel_grad = lax.psum(local_grad, 'fs')  100 us
    reduce_scatter x1, waiting for transfers between devices, body(): lax.psum_scatter(upper_term + lower_term, 'fs', scatter_dimension=0, tile...  78.8 us
    unnamed x28, local copies, waits for them, and re-layouts  4.95 us
    ppermute x1, starting transfers between devices, from_behind(): return lax.ppermute(x, axis, pairs)  4.87 us
  transfers between devices with their start and end apart: 4, of which 3 were waited for; matrix products, arithmetic and copies ran while one was open for 5% of the time, Pallas kernels for 0%

commit v1 on v0

v1 whole, which is shorter than its diff:
```python
import functools

import jax
import jax.numpy as jnp
from jax import lax
from jax.experimental import pallas as pl
from jax.experimental.pallas import tpu as pltpu
from jax.sharding import PartitionSpec as P

MESH = pl.DeviceIdType.MESH
LANES = 128
f32 = jnp.float32
bf16 = jnp.bfloat16


def remote(src, dst, send, recv, axis, peer):
    return pltpu.make_async_remote_copy(
        src_ref=src,
        dst_ref=dst,
        send_sem=send,
        recv_sem=recv,
        device_id={axis: peer},
        device_id_type=MESH,
    )


def reduce_kernel(
    n,
    m,
    x_ref,
    v_ref,
    g_ref,
    c_ref,
    f_ref,
    m1_ref,
    m2_ref,
    proj_ref,
    kg_ref,
    dn_ref,
    low_out,
    low_in,
    gram,
    part,
    recv,
    halo,
    ext,
    cot,
    stage,
    tap_out,
    tap_in,
    tap_all,
    dirs,
    low_s,
    low_r,
    gram_s,
    gram_r,
    bulk_s,
    bulk_r,
    halo_s,
    halo_r,
    tap_s,
    tap_r,
    all_s,
    all_r,
    dir_s,
    dir_r,
):
    me = lax.axis_index("fs")
    my = lax.axis_index("tp")
    tokens = x_ref.shape[0]
    width = f_ref.shape[0] * m
    rows, cols = m1_ref.shape
    reach = halo.shape[0]
    groups = ext.shape[0]
    taps = kg_ref.shape[0]
    padded = stage.shape[0] // groups

    def peers(count, own, fn):
        def step(off, carry):
            fn(off, lax.rem(own + off, count))
            return carry

        lax.fori_loop(1, count, step, 0)

    barrier = pltpu.get_barrier_semaphore()
    peers(n, me, lambda off, p: pl.semaphore_signal(barrier, inc=1, device_id={"fs": p}, device_id_type=MESH))
    peers(m, my, lambda off, p: pl.semaphore_signal(barrier, inc=1, device_id={"tp": p}, device_id_type=MESH))

    low = jnp.dot(x_ref[...], f_ref[...], preferred_element_type=f32).astype(bf16)
    for j in range(m):
        low_out[j] = low[:, j * cols : (j + 1) * cols]

    pl.semaphore_wait(barrier, n - 1 + m - 1)

    def low_copy(off, p):
        return remote(low_out.at[p], low_in.at[my], low_s.at[off], low_r.at[off], "tp", p)

    peers(m, my, lambda off, p: low_copy(off, p).start())
    low_in[my] = low_out[my]
    after = lax.rem(me + 1, n)
    halo_copy = remote(
        g_ref.at[pl.ds(tokens - reach, reach)], halo, halo_s, halo_r, "fs", after
    )
    halo_copy.start()

    peers(m, my, lambda off, p: low_copy(off, p).wait())
    reduced = low_in[0].astype(f32)
    for j in range(1, m):
        reduced = reduced + low_in[j].astype(f32)
    reduced = reduced.astype(bf16)

    part[...] = (
        lax.dot_general(v_ref[...], reduced, (((0,), (0,)), ((), ())), preferred_element_type=f32)
        .astype(bf16)
        .reshape(n, rows, cols)
    )

    def bulk_copy(off, p):
        return remote(part.at[p], recv.at[me], bulk_s.at[off], bulk_r.at[off], "fs", p)

    peers(n, me, lambda off, p: bulk_copy(off, p).start())
    recv[me] = part[me]

    halo_copy.wait()
    halo_f = jnp.where(me > 0, halo[...].astype(f32), 0.0)
    for g in range(groups):
        lanes = slice(g * LANES, (g + 1) * LANES)
        ext[g, :reach] = halo_f[:, lanes]
        ext[g, reach:] = g_ref[:, lanes].astype(f32)
        cot[g] = c_ref[:, lanes].astype(f32)

    def group_step(g, carry):
        right = cot[g]
        sums = []
        for k in range(taps):
            product = ext[g, pl.ds(reach - k, tokens), :] * right
            sums.append(jnp.sum(product, axis=0, keepdims=True))
        sums.append(jnp.zeros((padded - taps, LANES), f32))
        stage[pl.ds(pl.multiple_of(g * padded, padded), padded), :] = jnp.concatenate(sums, axis=0)
        return carry

    lax.fori_loop(0, groups, group_step, 0)
    tap_out[...] = stage[...].reshape(tap_out.shape).astype(bf16)

    def tap_copy(off, p):
        return remote(tap_out.at[p], tap_in.at[me], tap_s.at[off], tap_r.at[off], "fs", p)

    peers(n, me, lambda off, p: tap_copy(off, p).start())
    tap_in[me] = tap_out[me]

    gram[my] = lax.dot_general(
        f_ref[...], f_ref[...], (((0,), (0,)), ((), ())), preferred_element_type=f32
    )

    def gram_copy(off, p):
        return remote(gram.at[my], gram.at[my], gram_s.at[off], gram_r.at[off], "tp", p)

    peers(m, my, lambda off, p: gram_copy(off, p).start())

    peers(n, me, lambda off, p: bulk_copy(off, p).wait())
    projected = recv[0].astype(f32)
    for j in range(1, n):
        projected = projected + recv[j].astype(f32)
    proj_ref[...] = projected
    first = 0.8 * m1_ref[...] + 0.2 * projected
    second = 0.9 * m2_ref[...] + 0.1 * projected * projected
    dirs[my] = first / jnp.sqrt(second)

    def dir_copy(off, p):
        return remote(dirs.at[my], dirs.at[my], dir_s.at[off], dir_r.at[off], "tp", p)

    peers(m, my, lambda off, p: dir_copy(off, p).start())

    peers(n, me, lambda off, p: tap_copy(off, p).wait())
    tap_all[me] = jnp.sum(tap_in[...].astype(f32), axis=0).astype(bf16)

    def all_copy(off, p):
        return remote(tap_all.at[me], tap_all.at[me], all_s.at[off], all_r.at[off], "fs", p)

    peers(n, me, lambda off, p: all_copy(off, p).start())

    peers(m, my, lambda off, p: gram_copy(off, p).wait())
    total = gram[0]
    for j in range(1, m):
        total = total + gram[j]
    peers(m, my, lambda off, p: dir_copy(off, p).wait())
    direction = jnp.concatenate([dirs[j] for j in range(m)], axis=1)
    turned = jnp.dot(direction, total, precision=lax.Precision.HIGHEST, preferred_element_type=f32)
    mean = jnp.sum(turned * direction, axis=1, keepdims=True) / width
    dn_ref[...] = direction / jnp.sqrt(mean + 0.01)

    peers(n, me, lambda off, p: all_copy(off, p).wait())
    stage[...] = tap_all[...].astype(f32).reshape(stage.shape)
    for g in range(groups):
        kg_ref[:, g * LANES : (g + 1) * LANES] = stage[g * padded : g * padded + taps, :]


def update_kernel(
    dn_ref,
    f_ref,
    w_ref,
    proj_ref,
    m1_ref,
    m2_ref,
    kg_ref,
    k_ref,
    k1_ref,
    k2_ref,
    value_ref,
    copy_ref,
    step_ref,
    n1_ref,
    n2_ref,
    nk_ref,
    nk1_ref,
    nk2_ref,
):
    dn = dn_ref[...]
    upper = dn.astype(bf16)
    lower = (dn - upper.astype(f32)).astype(bf16)
    factor = f_ref[...]
    dims = (((1,), (1,)), ((), ()))
    step = lax.dot_general(upper, factor, dims, preferred_element_type=f32)
    step = step + lax.dot_general(lower, factor, dims, preferred_element_type=f32)
    step_ref[...] = step
    value = w_ref[...] - 0.05 * step
    value_ref[...] = value
    copy_ref[...] = value.astype(bf16)

    @pl.when(pl.program_id(0) == 0)
    def _():
        projected = proj_ref[...]
        n1_ref[...] = 0.8 * m1_ref[...] + 0.2 * projected
        n2_ref[...] = 0.9 * m2_ref[...] + 0.1 * projected * projected
        grad = kg_ref[...]
        first = 0.8 * k1_ref[...] + 0.2 * grad
        second = 0.9 * k2_ref[...] + 0.1 * grad * grad
        nk1_ref[...] = first
        nk2_ref[...] = second
        nk_ref[...] = k_ref[...] - 0.05 * first / jnp.sqrt(second)


def body(n, m, x, v, g, c, f, w, m1, m2, k, k1, k2):
    tokens = x.shape[0]
    features, rank = f.shape
    rows, cols = m1.shape
    taps, channels = k.shape
    groups = channels // LANES
    reach = -(-(taps - 1) // 16) * 16
    padded = -(-taps // 8) * 8
    chunk = groups * padded // n
    vmem = pl.BlockSpec(memory_space=pltpu.VMEM)
    dma = pltpu.SemaphoreType.DMA
    proj, kg, dn = pl.pallas_call(
        functools.partial(reduce_kernel, n, m),
        out_shape=(
            jax.ShapeDtypeStruct((rows, cols), f32),
            jax.ShapeDtypeStruct((taps, channels), f32),
            jax.ShapeDtypeStruct((rows, rank), f32),
        ),
        in_specs=[vmem] * 7,
        out_specs=(vmem,) * 3,
        scratch_shapes=[
            pltpu.VMEM((m, tokens, cols), bf16),
            pltpu.VMEM((m, tokens, cols), bf16),
            pltpu.VMEM((m, rank, rank), f32),
            pltpu.VMEM((n, rows, cols), bf16),
            pltpu.VMEM((n, rows, cols), bf16),
            pltpu.VMEM((reach, channels), bf16),
            pltpu.VMEM((groups, reach + tokens, LANES), f32),
            pltpu.VMEM((groups, tokens, LANES), f32),
            pltpu.VMEM((groups * padded, LANES), f32),
            pltpu.VMEM((n, chunk, LANES), bf16),
            pltpu.VMEM((n, chunk, LANES), bf16),
            pltpu.VMEM((n, chunk, LANES), bf16),
            pltpu.VMEM((m, rows, cols), f32),
            dma((m,)),
            dma((m,)),
            dma((m,)),
            dma((m,)),
            dma((n,)),
            dma((n,)),
            dma,
            dma,
            dma((n,)),
            dma((n,)),
            dma((n,)),
            dma((n,)),
            dma((m,)),
            dma((m,)),
        ],
        compiler_params=pltpu.CompilerParams(collective_id=0, has_side_effects=True),
        name="reduce",
    )(x, v, g, c, f, m1, m2)

    steps = 4 if features % (4 * LANES) == 0 else 1
    block = features // steps
    whole = lambda a: pl.BlockSpec(a.shape, lambda i: (0, 0))
    wide = pl.BlockSpec((rows, block), lambda i: (0, i))
    return pl.pallas_call(
        update_kernel,
        grid=(steps,),
        out_shape=(
            jax.ShapeDtypeStruct(w.shape, f32),
            jax.ShapeDtypeStruct(w.shape, bf16),
            jax.ShapeDtypeStruct(w.shape, f32),
            jax.ShapeDtypeStruct(m1.shape, f32),
            jax.ShapeDtypeStruct(m1.shape, f32),
            jax.ShapeDtypeStruct(k.shape, f32),
            jax.ShapeDtypeStruct(k.shape, f32),
            jax.ShapeDtypeStruct(k.shape, f32),
        ),
        in_specs=[
            whole(dn),
            pl.BlockSpec((block, rank), lambda i: (i, 0)),
            wide,
            whole(proj),
            whole(m1),
            whole(m2),
            whole(kg),
            whole(k),
            whole(k1),
            whole(k2),
        ],
        out_specs=(wide, wide, wide, whole(m1), whole(m1), whole(k), whole(k), whole(k)),
        compiler_params=pltpu.CompilerParams(dimension_semantics=("arbitrary",)),
        name="update",
    )(dn, f, w, proj, m1, m2, kg, k, k1, k2)


def solution(mesh):
    both, rows, cols = P("fs", "tp"), P("fs", None), P(None, "tp")
    return jax.shard_map(
        functools.partial(body, mesh.shape["fs"], mesh.shape["tp"]),
        mesh=mesh,
        in_specs=(both, rows, both, both, P("tp", None), both, both, both, cols, cols, cols),
        out_specs=(both, both, both, both, both, cols, cols, cols),
        check_vma=False,
    )
```

time: 226 us -> 37.7 us (0.17)
  waiting for transfers between devices: 181 us -> 0 us
  Pallas kernels: 0 us -> 36.9 us
  between operations: 15.6 us -> 0.64 us
  local copies, waits for them, and re-layouts: 8.54 us -> 0 us
  other arithmetic: 6.33 us -> 0 us
  starting transfers between devices: 5 us -> 0 us
  blocking collectives: 4.37 us -> 0 us
  matrix products: 4.05 us -> 0 us
    psum x1 -> x0, waiting for transfers between devices: 100 us -> none  [body(): kernel_grad = lax.psum(local_grad, 'fs')]
    reduce_scatter x1 -> x0, waiting for transfers between devices: 78.8 us -> none  [body(): lax.psum_scatter(upper_term + lower_term, 'fs', scatter_dimension=0, tile...]
    pallas_call x0 -> x2, Pallas kernels: none -> 36.9 us  [the longest x1 31.9 us: body(): pl.pallas_call(functools.partial(reduce_kernel, n, m), out_shape=(jax.Sha...]
    unnamed x28 -> x0, local copies, waits for them, and re-layouts: 4.95 us -> none
    ppermute x1 -> x0, starting transfers between devices: 4.87 us -> none  [from_behind(): return lax.ppermute(x, axis, pairs)]
    dot_general x4 -> x0, matrix products: 4.05 us -> none  [the longest x1 1.39 us: body(): jnp.dot(saved_inputs, factor, preferred_element_type=jnp.float32)]
    another operation x1 -> x0, local copies, waits for them, and re-layouts: 2.66 us -> none  [body(): local_grad = jnp.stack(pieces, axis=0)]
    psum x1 -> x0, blocking collectives: 2.47 us -> none  [body(): row_squares = lax.psum(jnp.sum(back_proj * back_proj, axis=1), 'tp')]
  transfers between devices with their start and end apart: 4 -> 0, of which waited for: 3 -> 0; matrix products, arithmetic and copies ran while one was open for 5% -> 0% of each run, Pallas kernels for 0% -> 0%
where the time goes in v1:
time: 37.7 us; the launch traced here: 37.5 us
  Pallas kernels  36.9 us (98%)
  between operations  0.64 us (2%)
    pallas_call x1, Pallas kernels, body(): pl.pallas_call(functools.partial(reduce_kernel, n, m), out_shape=(jax.Sha...  31.9 us
    pallas_call x1, Pallas kernels, body(): pl.pallas_call(update_kernel, grid=(steps,), out_shape=(jax.ShapeDtypeStr...  4.99 us

profile of v1, /device:TPU:0, one launch (start us, length us, event | category | flops | bytes accessed | tf_op | source)
XLA Modules:
  0.0 37.5 jit_solution(18072425398944591814)
XLA Ops:
  0.6 31.9 %reduce.1 = (f32[128,128]{1,0:T(8,128)}, f32[31,1024]{1,0:T(8,128)}, f32[128,256]{1,0:T(8,128)}) custom-call(bf16[128,2048]{1,0:T(8,128)(2,1)} %x_ref.1, bf16[128,2048]{1,0:T(8,128)(2,1)} %v_ref.1, bf16[128,1024]{1,0:T(8,128)(2,1)} %g_ref.1, bf16[128,1024]{1,0:T(8,128)(2,1)} %c_ref.1, bf16[2048,256]{1,0:T(8,128)(2,1)} %f_ref.3, f32[128,128]{1,0:T(8,128)} %m1_ref.3, ...), custom_call_target="tpu_custom_call" | custom-call | tf_op jit(solution)/shard_map/reduce/pallas_call | solution.py:254
  32.5 5.0 %update.1 = (f32[128,2048]{1,0:T(8,128)}, bf16[128,2048]{1,0:T(8,128)(2,1)}, f32[128,2048]{1,0:T(8,128)}, f32[128,128]{1,0:T(8,128)}, f32[128,128]{1,0:T(8,128)}...) custom-call(f32[128,256]{1,0:T(8,128)} %get-tuple-element.11.dn_ref, bf16[2048,256]{1,0:T(8,128)(2,1)} %f_ref.3, ...), custom_call_target="tpu_custom_call" | custom-call | tf_op jit(solution)/shard_map/update/pallas_call | solution.py:300

commit v2 on v1

--- a/solution.py
+++ b/solution.py
@@ -27,6 +27,16 @@
 def reduce_kernel(
     n,
     m,
+    x_hbm,
+    v_hbm,
+    g_hbm,
+    c_hbm,
+    f_hbm,
+    m1_hbm,
+    m2_hbm,
+    proj_ref,
+    kg_ref,
+    dn_ref,
     x_ref,
     v_ref,
     g_ref,
@@ -34,9 +44,7 @@
     f_ref,
     m1_ref,
     m2_ref,
-    proj_ref,
-    kg_ref,
-    dn_ref,
+    load_s,
     low_out,
     low_in,
     gram,
@@ -86,9 +94,42 @@
     peers(n, me, lambda off, p: pl.semaphore_signal(barrier, inc=1, device_id={"fs": p}, device_id_type=MESH))
     peers(m, my, lambda off, p: pl.semaphore_signal(barrier, inc=1, device_id={"tp": p}, device_id_type=MESH))
 
+    pairs = [(x_hbm, x_ref), (f_hbm, f_ref), (g_hbm, g_ref), (c_hbm, c_ref)]
+    pairs += [(v_hbm, v_ref), (m1_hbm, m1_ref), (m2_hbm, m2_ref)]
+    loads = [pltpu.make_async_copy(a, b, load_s.at[i]) for i, (a, b) in enumerate(pairs)]
+    for load in loads:
+        load.start()
+    loads[0].wait()
+    loads[1].wait()
+
     low = jnp.dot(x_ref[...], f_ref[...], preferred_element_type=f32).astype(bf16)
     for j in range(m):
         low_out[j] = low[:, j * cols : (j + 1) * cols]
+
+    loads[2].wait()
+    loads[3].wait()
+    for g in range(groups):
+        lanes = slice(g * LANES, (g + 1) * LANES)
+        ext[g, :reach] = jnp.zeros((reach, LANES), f32)
+        ext[g, reach:] = g_ref[:, lanes].astype(f32)
+        cot[g] = c_ref[:, lanes].astype(f32)
+
+    def group_step(count, add):
+        def step(g, carry):
+            right = cot[g, :count, :]
+            sums = []
+            for k in range(taps):
+                product = ext[g, pl.ds(reach - k, count), :] * right
+                sums.append(jnp.sum(product, axis=0, keepdims=True))
+            sums.append(jnp.zeros((padded - taps, LANES), f32))
+            at = pl.ds(pl.multiple_of(g * padded, padded), padded)
+            block = jnp.concatenate(sums, axis=0)
+            stage[at, :] = stage[at, :] + block if add else block
+            return carry
+
+        lax.fori_loop(0, groups, step, 0)
+
+    group_step(tokens, False)
 
     pl.semaphore_wait(barrier, n - 1 + m - 1)
 
@@ -103,6 +144,21 @@
     )
     halo_copy.start()
 
+    halo_copy.wait()
+    halo_f = jnp.where(me > 0, halo[...].astype(f32), 0.0)
+    for g in range(groups):
+        ext[g, :reach] = halo_f[:, g * LANES : (g + 1) * LANES]
+        ext[g, reach:] = jnp.zeros((tokens, LANES), f32)
+    group_step(reach, True)
+    tap_out[...] = stage[...].reshape(tap_out.shape).astype(bf16)
+
+    def tap_copy(off, p):
+        return remote(tap_out.at[p], tap_in.at[me], tap_s.at[off], tap_r.at[off], "fs", p)
+
+    peers(n, me, lambda off, p: tap_copy(off, p).start())
+    tap_in[me] = tap_out[me]
+    loads[4].wait()
+
     peers(m, my, lambda off, p: low_copy(off, p).wait())
     reduced = low_in[0].astype(f32)
     for j in range(1, m):
@@ -121,33 +177,6 @@
     peers(n, me, lambda off, p: bulk_copy(off, p).start())
     recv[me] = part[me]
 
-    halo_copy.wait()
-    halo_f = jnp.where(me > 0, halo[...].astype(f32), 0.0)
-    for g in range(groups):
-        lanes = slice(g * LANES, (g + 1) * LANES)
-        ext[g, :reach] = halo_f[:, lanes]
-        ext[g, reach:] = g_ref[:, lanes].astype(f32)
-        cot[g] = c_ref[:, lanes].astype(f32)
-
-    def group_step(g, carry):
-        right = cot[g]
-        sums = []
-        for k in range(taps):
-            product = ext[g, pl.ds(reach - k, tokens), :] * right
-            sums.append(jnp.sum(product, axis=0, keepdims=True))
-        sums.append(jnp.zeros((padded - taps, LANES), f32))
-        stage[pl.ds(pl.multiple_of(g * padded, padded), padded), :] = jnp.concatenate(sums, axis=0)
-        return carry
-
-    lax.fori_loop(0, groups, group_step, 0)
-    tap_out[...] = stage[...].reshape(tap_out.shape).astype(bf16)
-
-    def tap_copy(off, p):
-        return remote(tap_out.at[p], tap_in.at[me], tap_s.at[off], tap_r.at[off], "fs", p)
-
-    peers(n, me, lambda off, p: tap_copy(off, p).start())
-    tap_in[me] = tap_out[me]
-
     gram[my] = lax.dot_general(
         f_ref[...], f_ref[...], (((0,), (0,)), ((), ())), preferred_element_type=f32
     )
@@ -157,6 +186,16 @@
 
     peers(m, my, lambda off, p: gram_copy(off, p).start())
 
+    peers(n, me, lambda off, p: tap_copy(off, p).wait())
+    tap_all[me] = jnp.sum(tap_in[...].astype(f32), axis=0).astype(bf16)
+
+    def all_copy(off, p):
+        return remote(tap_all.at[me], tap_all.at[me], all_s.at[off], all_r.at[off], "fs", p)
+
+    peers(n, me, lambda off, p: all_copy(off, p).start())
+
+    loads[5].wait()
+    loads[6].wait()
     peers(n, me, lambda off, p: bulk_copy(off, p).wait())
     projected = recv[0].astype(f32)
     for j in range(1, n):
@@ -171,14 +210,6 @@
 
     peers(m, my, lambda off, p: dir_copy(off, p).start())
 
-    peers(n, me, lambda off, p: tap_copy(off, p).wait())
-    tap_all[me] = jnp.sum(tap_in[...].astype(f32), axis=0).astype(bf16)
-
-    def all_copy(off, p):
-        return remote(tap_all.at[me], tap_all.at[me], all_s.at[off], all_r.at[off], "fs", p)
-
-    peers(n, me, lambda off, p: all_copy(off, p).start())
-
     peers(m, my, lambda off, p: gram_copy(off, p).wait())
     total = gram[0]
     for j in range(1, m):
@@ -187,7 +218,7 @@
     direction = jnp.concatenate([dirs[j] for j in range(m)], axis=1)
     turned = jnp.dot(direction, total, precision=lax.Precision.HIGHEST, preferred_element_type=f32)
     mean = jnp.sum(turned * direction, axis=1, keepdims=True) / width
-    dn_ref[...] = direction / jnp.sqrt(mean + 0.01)
+    dn_ref[...] = (direction / jnp.sqrt(mean + 0.01)).astype(bf16)
 
     peers(n, me, lambda off, p: all_copy(off, p).wait())
     stage[...] = tap_all[...].astype(f32).reshape(stage.shape)
@@ -215,13 +246,8 @@
     nk1_ref,
     nk2_ref,
 ):
-    dn = dn_ref[...]
-    upper = dn.astype(bf16)
-    lower = (dn - upper.astype(f32)).astype(bf16)
-    factor = f_ref[...]
     dims = (((1,), (1,)), ((), ()))
-    step = lax.dot_general(upper, factor, dims, preferred_element_type=f32)
-    step = step + lax.dot_general(lower, factor, dims, preferred_element_type=f32)
+    step = lax.dot_general(dn_ref[...], f_ref[...], dims, preferred_element_type=f32)
     step_ref[...] = step
     value = w_ref[...] - 0.05 * step
     value_ref[...] = value
@@ -256,11 +282,13 @@
         out_shape=(
             jax.ShapeDtypeStruct((rows, cols), f32),
             jax.ShapeDtypeStruct((taps, channels), f32),
-            jax.ShapeDtypeStruct((rows, rank), f32),
+            jax.ShapeDtypeStruct((rows, rank), bf16),
         ),
-        in_specs=[vmem] * 7,
+        in_specs=[pl.BlockSpec(memory_space=pl.ANY)] * 7,
         out_specs=(vmem,) * 3,
         scratch_shapes=[
+            *(pltpu.VMEM(a.shape, a.dtype) for a in (x, v, g, c, f, m1, m2)),
+            dma((7,)),
             pltpu.VMEM((m, tokens, cols), bf16),
             pltpu.VMEM((m, tokens, cols), bf16),
             pltpu.VMEM((m, rank, rank), f32),

time: 37.7 us -> 34.1 us (0.905)
  Pallas kernels: 36.9 us -> 33.2 us
    pallas_call x1, Pallas kernels: 31.9 us -> 28.4 us  [body(): pl.pallas_call(functools.partial(reduce_kernel, n, m), out_shape=(jax.Sha...]
where the time goes in v2:
time: 34.1 us; the launch traced here: 33.9 us
  Pallas kernels  33.2 us (97%)
  between operations  0.64 us (2%)
    pallas_call x1, Pallas kernels, body(): pl.pallas_call(functools.partial(reduce_kernel, n, m), out_shape=(jax.Sha...  28.4 us
    pallas_call x1, Pallas kernels, body(): pl.pallas_call(update_kernel, grid=(steps,), out_shape=(jax.ShapeDtypeStr...  4.8 us

profile of v2, /device:TPU:0, one launch (start us, length us, event | category | flops | bytes accessed | tf_op | source)
XLA Modules:
  0.0 33.9 jit_solution(8537564689506815954)
XLA Ops:
  0.6 28.4 %reduce.1 = (f32[128,128]{1,0:T(8,128)}, f32[31,1024]{1,0:T(8,128)}, bf16[128,256]{1,0:T(8,128)(2,1)}) custom-call(bf16[128,2048]{1,0:T(8,128)(2,1)} %x_hbm.1, bf16[128,2048]{1,0:T(8,128)(2,1)} %v_hbm.1, bf16[128,1024]{1,0:T(8,128)(2,1)} %g_hbm.1, bf16[128,1024]{1,0:T(8,128)(2,1)} %c_hbm.1, bf16[2048,256]{1,0:T(8,128)(2,1)} %f_ref.1, f32[128,128]{1,0:T(8,128)} %m1_ref.1, ...), custom_call_target="tpu_custom_call" | custom-call | tf_op jit(solution)/shard_map/reduce/pallas_call | solution.py:280
  29.1 4.8 %update.1 = (f32[128,2048]{1,0:T(8,128)}, bf16[128,2048]{1,0:T(8,128)(2,1)}, f32[128,2048]{1,0:T(8,128)}, f32[128,128]{1,0:T(8,128)}, f32[128,128]{1,0:T(8,128)}...) custom-call(bf16[128,256]{1,0:T(8,128)(2,1)} %get-tuple-element.11.dn_ref, bf16[2048,256]{1,0:T(8,128)(2,1)} %f_ref.1, ...), custom_call_target="tpu_custom_call" | custom-call | tf_op jit(solution)/shard_map/update/pallas_call | solution.py:328

commit v3 on v2

--- a/solution.py
+++ b/solution.py
@@ -90,6 +90,21 @@
 
         lax.fori_loop(1, count, step, 0)
 
+    def far_first(fn):
+        half = n // 2
+        side, place = me // half, lax.rem(me, half)
+
+        def across(j, carry):
+            fn(j, (1 - side) * half + lax.rem(place + j, half))
+            return carry
+
+        def along(j, carry):
+            fn(half + j, side * half + lax.rem(place + j, half))
+            return carry
+
+        lax.fori_loop(0, half, across, 0)
+        lax.fori_loop(1, half, along, 0)
+
     barrier = pltpu.get_barrier_semaphore()
     peers(n, me, lambda off, p: pl.semaphore_signal(barrier, inc=1, device_id={"fs": p}, device_id_type=MESH))
     peers(m, my, lambda off, p: pl.semaphore_signal(barrier, inc=1, device_id={"tp": p}, device_id_type=MESH))
@@ -174,7 +189,7 @@
     def bulk_copy(off, p):
         return remote(part.at[p], recv.at[me], bulk_s.at[off], bulk_r.at[off], "fs", p)
 
-    peers(n, me, lambda off, p: bulk_copy(off, p).start())
+    far_first(lambda off, p: bulk_copy(off, p).start())
     recv[me] = part[me]
 
     gram[my] = lax.dot_general(
@@ -196,7 +211,7 @@
 
     loads[5].wait()
     loads[6].wait()
-    peers(n, me, lambda off, p: bulk_copy(off, p).wait())
+    far_first(lambda off, p: bulk_copy(off, p).wait())
     projected = recv[0].astype(f32)
     for j in range(1, n):
         projected = projected + recv[j].astype(f32)
@@ -226,44 +241,58 @@
         kg_ref[:, g * LANES : (g + 1) * LANES] = stage[g * padded : g * padded + taps, :]
 
 
-def update_kernel(
-    dn_ref,
-    f_ref,
-    w_ref,
-    proj_ref,
-    m1_ref,
-    m2_ref,
-    kg_ref,
-    k_ref,
-    k1_ref,
-    k2_ref,
-    value_ref,
-    copy_ref,
-    step_ref,
-    n1_ref,
-    n2_ref,
-    nk_ref,
-    nk1_ref,
-    nk2_ref,
-):
+def update_kernel(steps, *refs):
+    source, target, local, made = refs[:10], refs[10:18], refs[18:28], refs[28:36]
+    small_s, f_s, w_s, out_s, wide_s = refs[36:]
+    dn_ref, f_ref, w_ref, proj_ref, m1_ref, m2_ref, kg_ref, k_ref, k1_ref, k2_ref = local
+    value_ref, copy_ref, step_ref, n1_ref, n2_ref, nk_ref, nk1_ref, nk2_ref = made
+    block = f_ref.shape[0] // steps
+    spans = [pl.ds(i * block, block) for i in range(steps)]
+    copy = pltpu.make_async_copy
+    small = {i: copy(source[i], local[i], small_s.at[i]) for i in (0, 3, 4, 5, 6, 7, 8, 9)}
+    f_in = [copy(source[1].at[at], f_ref.at[at], f_s.at[i]) for i, at in enumerate(spans)]
+    w_in = [copy(source[2].at[:, at], w_ref.at[:, at], w_s.at[i]) for i, at in enumerate(spans)]
+    small[0].start()
+    for i in range(steps):
+        f_in[i].start()
+        w_in[i].start()
+    for i in range(3, 10):
+        small[i].start()
+
+    outs = []
     dims = (((1,), (1,)), ((), ()))
-    step = lax.dot_general(dn_ref[...], f_ref[...], dims, preferred_element_type=f32)
-    step_ref[...] = step
-    value = w_ref[...] - 0.05 * step
-    value_ref[...] = value
-    copy_ref[...] = value.astype(bf16)
-
-    @pl.when(pl.program_id(0) == 0)
-    def _():
-        projected = proj_ref[...]
-        n1_ref[...] = 0.8 * m1_ref[...] + 0.2 * projected
-        n2_ref[...] = 0.9 * m2_ref[...] + 0.1 * projected * projected
-        grad = kg_ref[...]
-        first = 0.8 * k1_ref[...] + 0.2 * grad
-        second = 0.9 * k2_ref[...] + 0.1 * grad * grad
-        nk1_ref[...] = first
-        nk2_ref[...] = second
-        nk_ref[...] = k_ref[...] - 0.05 * first / jnp.sqrt(second)
+    small[0].wait()
+    dn = dn_ref[...]
+    for i, at in enumerate(spans):
+        f_in[i].wait()
+        step = lax.dot_general(dn, f_ref[at, :], dims, preferred_element_type=f32)
+        w_in[i].wait()
+        step_ref[:, at] = step
+        value = w_ref[:, at] - 0.05 * step
+        value_ref[:, at] = value
+        copy_ref[:, at] = value.astype(bf16)
+        for j in range(3):
+            out = copy(made[j].at[:, at], target[j].at[:, at], wide_s.at[j, i])
+            out.start()
+            outs.append(out)
+
+    for i in range(3, 10):
+        small[i].wait()
+    projected = proj_ref[...]
+    n1_ref[...] = 0.8 * m1_ref[...] + 0.2 * projected
+    n2_ref[...] = 0.9 * m2_ref[...] + 0.1 * projected * projected
+    grad = kg_ref[...]
+    first = 0.8 * k1_ref[...] + 0.2 * grad
+    second = 0.9 * k2_ref[...] + 0.1 * grad * grad
+    nk1_ref[...] = first
+    nk2_ref[...] = second
+    nk_ref[...] = k_ref[...] - 0.05 * first / jnp.sqrt(second)
+    for j in range(3, 8):
+        out = copy(made[j], target[j], out_s.at[j])
+        out.start()
+        outs.append(out)
+    for out in outs:
+        out.wait()
 
 
 def body(n, m, x, v, g, c, f, w, m1, m2, k, k1, k2):
@@ -322,38 +351,34 @@
     )(x, v, g, c, f, m1, m2)
 
     steps = 4 if features % (4 * LANES) == 0 else 1
-    block = features // steps
-    whole = lambda a: pl.BlockSpec(a.shape, lambda i: (0, 0))
-    wide = pl.BlockSpec((rows, block), lambda i: (0, i))
+    operands = (dn, f, w, proj, m1, m2, kg, k, k1, k2)
+    results = (
+        jax.ShapeDtypeStruct(w.shape, f32),
+        jax.ShapeDtypeStruct(w.shape, bf16),
+        jax.ShapeDtypeStruct(w.shape, f32),
+        jax.ShapeDtypeStruct(m1.shape, f32),
+        jax.ShapeDtypeStruct(m1.shape, f32),
+        jax.ShapeDtypeStruct(k.shape, f32),
+        jax.ShapeDtypeStruct(k.shape, f32),
+        jax.ShapeDtypeStruct(k.shape, f32),
+    )
+    hbm = pl.BlockSpec(memory_space=pl.ANY)
     return pl.pallas_call(
-        update_kernel,
-        grid=(steps,),
-        out_shape=(
-            jax.ShapeDtypeStruct(w.shape, f32),
-            jax.ShapeDtypeStruct(w.shape, bf16),
-            jax.ShapeDtypeStruct(w.shape, f32),
-            jax.ShapeDtypeStruct(m1.shape, f32),
-            jax.ShapeDtypeStruct(m1.shape, f32),
-            jax.ShapeDtypeStruct(k.shape, f32),
-            jax.ShapeDtypeStruct(k.shape, f32),
-            jax.ShapeDtypeStruct(k.shape, f32),
-        ),
-        in_specs=[
-            whole(dn),
-            pl.BlockSpec((block, rank), lambda i: (i, 0)),
-            wide,
-            whole(proj),
-            whole(m1),
-            whole(m2),
-            whole(kg),
-            whole(k),
-            whole(k1),
-            whole(k2),
+        functools.partial(update_kernel, steps),
+        out_shape=results,
+        in_specs=[hbm] * 10,
+        out_specs=(hbm,) * 8,
+        scratch_shapes=[
+            *(pltpu.VMEM(a.shape, a.dtype) for a in operands),
+            *(pltpu.VMEM(a.shape, a.dtype) for a in results),
+            dma((10,)),
+            dma((steps,)),
+            dma((steps,)),
+            dma((8,)),
+            dma((3, steps)),
         ],
-        out_specs=(wide, wide, wide, whole(m1), whole(m1), whole(k), whole(k), whole(k)),
-        compiler_params=pltpu.CompilerParams(dimension_semantics=("arbitrary",)),
         name="update",
-    )(dn, f, w, proj, m1, m2, kg, k, k1, k2)
+    )(*operands)
 
 
 def solution(mesh):

time: 34.1 us -> 33.8 us (level)
    pallas_call x1, Pallas kernels: 4.8 us -> 3.53 us  [body(): pl.pallas_call(functools.partial(update_kernel, steps), out_shape=results...]
    pallas_call x1, Pallas kernels: 28.4 us -> 29.5 us  [body(): pl.pallas_call(functools.partial(reduce_kernel, n, m), out_shape=(jax.Sha...]
where the time goes in v3:
time: 33.8 us; the launch traced here: 33.7 us
  Pallas kernels  33 us (98%)
  between operations  0.64 us (2%)
    pallas_call x1, Pallas kernels, body(): pl.pallas_call(functools.partial(reduce_kernel, n, m), out_shape=(jax.Sha...  29.5 us
    pallas_call x1, Pallas kernels, body(): pl.pallas_call(functools.partial(update_kernel, steps), out_shape=results...  3.53 us

profile of v3, /device:TPU:0, one launch (start us, length us, event | category | flops | bytes accessed | tf_op | source)
XLA Modules:
  0.0 33.7 jit_solution(12617890469747969151)
XLA Ops:
  0.6 29.5 %reduce.1 = (f32[128,128]{1,0:T(8,128)}, f32[31,1024]{1,0:T(8,128)}, bf16[128,256]{1,0:T(8,128)(2,1)}) custom-call(bf16[128,2048]{1,0:T(8,128)(2,1)} %x_hbm.1, bf16[128,2048]{1,0:T(8,128)(2,1)} %v_hbm.1, bf16[128,1024]{1,0:T(8,128)(2,1)} %g_hbm.1, bf16[128,1024]{1,0:T(8,128)(2,1)} %c_hbm.1, bf16[2048,256]{1,0:T(8,128)(2,1)} %refs_1_.1, f32[128,128]{1,0:T(8,128)} %refs_4_.1, ...), custom_call_target="tpu_custom_call" | custom-call | tf_op jit(solution)/shard_map/reduce/pallas_call | solution.py:309
  30.1 3.5 %update.1 = (f32[128,2048]{1,0:T(8,128)}, bf16[128,2048]{1,0:T(8,128)(2,1)}, f32[128,2048]{1,0:T(8,128)}, f32[128,128]{1,0:T(8,128)}, f32[128,128]{1,0:T(8,128)}...) custom-call(bf16[128,256]{1,0:T(8,128)(2,1)} %get-tuple-element.11.refs_0_, ...), custom_call_target="tpu_custom_call" | custom-call | tf_op jit(solution)/shard_map/update/pallas_call | solution.py:366
